TPU v7x, 32 devices: a whole 2x2x4 slice. The times are simulated.
32 devices in a mesh: sp: 8 (over z, x), tp: 4 (over y, core).
Axes of the slice: x: 2, y: 2, z: 4, core: 2. Of those that a mesh axis runs over, the one named last changes fastest.
Arguments:
- residual: bfloat16 [1024, 2048], P(('sp', 'tp')), may hold values from -6 to 6
- query_rows: bfloat16 [1024, 1024], P('sp', 'tp'), may hold values from -6 to 6
- key_rows: bfloat16 [1024, 512], P('sp', 'tp'), may hold values from -6 to 6
- value_rows: bfloat16 [1024, 512], P('sp', 'tp'), may hold values from -8 to 8
- head_offset: float32 [8], P('tp'), may hold values from -13 to -3
- w_out: bfloat16 [1024, 2048], P('tp'), may hold values from -0.5 to 0.5
- norm_gain: float32 [2, 2048], replicated, may hold values from 0.1 to 1.9
- norm_bias: float32 [2, 2048], replicated, may hold values from -1.5 to 1.5
- routing: int32 [1024, 2], P(('sp', 'tp')), may hold values from 0 to 7, all different within a row; in each aligned block of 32 rows (0 to 31, 32 to 63, ...) at most 12 rows name the same one
- route_weight: float32 [1024, 2], P(('sp', 'tp')), may hold values from 0.2 to 1
- w_exp_gate: bfloat16 [8, 2048, 1024], P('sp', None, 'tp'), may hold values from -0.125 to 0.125
- w_exp_up: bfloat16 [8, 2048, 1024], P('sp', None, 'tp'), may hold values from -0.125 to 0.125
- w_exp_down: bfloat16 [8, 1024, 2048], P('sp', 'tp'), may hold values from -0.1875 to 0.1875
- w_shared_gate: bfloat16 [2048, 1024], P(None, 'tp'), may hold values from -0.125 to 0.125
- w_shared_up: bfloat16 [2048, 1024], P(None, 'tp'), may hold values from -0.125 to 0.125
- w_shared_down: bfloat16 [1024, 2048], P('tp'), may hold values from -0.1875 to 0.1875
Outputs:
- result: bfloat16 [1024, 2048], P(('sp', 'tp'))
Inputs may be any that keep to these rules, and one draw needn't show every extreme that they name: `routing`: each row names 2 different experts; within the rows of one device (32 tokens) no expert is named by more than 12 of them, a bound that some block reaches.
All inputs are finite; a program needn't handle non-finite values.
Results may differ from a plain program's by a relative error of at most 0.013.
Values may be sent and summed in bfloat16 or wider, within the bound.
A program may use at most 64 MiB of HBM per device.

v0:
```python
import jax
import jax.numpy as jnp
from jax import lax
from jax.sharding import PartitionSpec as P

DH = 128


ALPHA = 8.0**0.25
LN_EPS = 1e-05


def layer_norm(summed, gain, shift):
    center = summed - jnp.mean(summed, axis=-1, keepdims=True)
    spread = jnp.mean(center * center, axis=-1, keepdims=True)
    return (center * lax.rsqrt(spread + LN_EPS) * gain + shift).astype(jnp.bfloat16)


def span_of():
    return 4


def stick_terms(queries, keys_block, key_start, query_pos, offset, shard_len):
    kv_local, group_size = offset.shape
    query_count = queries.shape[0]
    key_count = keys_block.shape[0]
    head_dim = keys_block.shape[-1]
    scores = jnp.einsum("tkgd,skd->kgts", queries, keys_block, preferred_element_type=jnp.float32)
    scores = scores * head_dim ** (-0.5) + offset[:, :, None, None]
    key_pos = key_start + jnp.arange(key_count, dtype=jnp.int32)
    causal = key_pos[None, :] < query_pos[:, None]
    leftover = jnp.where(causal, jax.nn.log_sigmoid(-scores), 0.0)
    shape_five = (kv_local, group_size, query_count, key_count // shard_len, shard_len)
    causal = causal.reshape(query_count, key_count // shard_len, shard_len)
    return (scores.reshape(shape_five), causal, leftover.reshape(shape_five))


def stick_block(queries, keys_block, values_block, key_start, query_pos, offset, shard_len, beyond):
    scores, causal, leftover = stick_terms(
        queries, keys_block, key_start, query_pos, offset, shard_len
    )
    within = lax.cumsum(leftover, axis=4, reverse=True) - leftover
    totals = jnp.sum(leftover, axis=4)
    exponent = jax.nn.log_sigmoid(scores) + within + beyond[..., None]
    weights = jnp.where(causal[None, None], jnp.exp(exponent), 0.0).astype(jnp.bfloat16)
    weights = weights.reshape(scores.shape[0], scores.shape[1], scores.shape[2], -1)
    partial_out = jnp.einsum(
        "kgts,skd->tkgd", weights, values_block, preferred_element_type=jnp.float32
    )
    return (partial_out, totals)


def per_device(
    residual,
    query_rows,
    key_rows,
    value_rows,
    head_offset,
    w_out,
    norm_gain,
    norm_bias,
    routing,
    route_weight,
    w_exp_gate,
    w_exp_up,
    w_exp_down,
    w_shared_gate,
    w_shared_up,
    w_shared_down,
):
    shard_len = query_rows.shape[0]
    kv_local = key_rows.shape[1] // DH
    heads_local = query_rows.shape[1] // DH
    group_size = heads_local // kv_local
    sp_count = lax.axis_size("sp")
    sp_index = lax.axis_index("sp")
    queries = query_rows.reshape(shard_len, kv_local, group_size, DH)
    offset = head_offset.reshape(kv_local, group_size)
    query_pos = sp_index * shard_len + jnp.arange(shard_len, dtype=jnp.int32)
    empty_out = jnp.zeros((shard_len, kv_local, group_size, DH), jnp.float32)
    empty_table = jnp.zeros((kv_local, group_size, shard_len, sp_count), jnp.float32)
    piece_rows = lax.all_gather(key_rows, "sp", axis=0, tiled=True)
    shard_count = piece_rows.shape[0] // shard_len
    span_len = span_of()
    keys_piece = piece_rows.reshape(-1, kv_local, DH)

    def sweep(step_index, table_now):
        first_key = step_index * span_len * shard_len
        keys_block = lax.dynamic_slice_in_dim(keys_piece, first_key, span_len * shard_len, 0)
        _, _, leftover = stick_terms(queries, keys_block, first_key, query_pos, offset, shard_len)
        return lax.dynamic_update_slice_in_dim(
            table_now, jnp.sum(leftover, axis=4), first_key // shard_len, 3
        )

    totals_table = lax.fori_loop(0, shard_count // span_len, sweep, empty_table)
    later_sum = lax.cumsum(totals_table, axis=3, reverse=True) - totals_table
    add_keys_piece = lax.all_gather(key_rows, "sp", axis=0, tiled=True).reshape(-1, kv_local, DH)
    values_piece = lax.all_gather(value_rows, "sp", axis=0, tiled=True).reshape(-1, kv_local, DH)
    shard_count = add_keys_piece.shape[0] // shard_len
    add_span_len = span_of()

    def sweep(step_index, out_now):
        first_key = step_index * add_span_len * shard_len
        keys_block = lax.dynamic_slice_in_dim(
            add_keys_piece, first_key, add_span_len * shard_len, 0
        )
        values_block = lax.dynamic_slice_in_dim(
            values_piece, first_key, add_span_len * shard_len, 0
        )
        beyond = lax.dynamic_slice_in_dim(later_sum, first_key // shard_len, add_span_len, 3)
        partial_out, _ = stick_block(
            queries, keys_block, values_block, first_key, query_pos, offset, shard_len, beyond
        )
        return out_now + partial_out

    attended = lax.fori_loop(0, shard_count // add_span_len, sweep, empty_out)
    attended = attended.astype(jnp.bfloat16).reshape(shard_len, heads_local * DH)
    rows_local = residual.shape[0]
    mixed = lax.psum_scatter(
        jnp.dot(attended, w_out, preferred_element_type=jnp.float32).astype(jnp.bfloat16),
        "tp",
        scatter_dimension=0,
        tiled=True,
    ).astype(jnp.float32)
    normed = layer_norm(ALPHA * residual.astype(jnp.float32) + mixed, norm_gain[0], norm_bias[0])
    top_k = routing.shape[1]
    exp_local = w_exp_gate.shape[0]
    experts = exp_local * sp_count
    capacity = max(2, 3 * rows_local * top_k // (2 * experts))
    flat_routes = routing.reshape(-1)
    one_hot = (flat_routes[:, None] == jnp.arange(experts, dtype=jnp.int32)[None, :]).astype(
        jnp.int32
    )
    slot_rank = jnp.sum((jnp.cumsum(one_hot, axis=0) - 1) * one_hot, axis=1)
    slot_index = flat_routes * capacity + slot_rank
    pair_token = jnp.arange(flat_routes.shape[0], dtype=jnp.int32) // top_k
    source_row = (
        jnp.full((experts * capacity,), rows_local, jnp.int32).at[slot_index].set(pair_token)
    )
    outgoing = jnp.take(normed, source_row, axis=0, mode="fill", fill_value=0)
    outgoing = outgoing.reshape(sp_count, exp_local, capacity, -1)
    arrived = lax.all_to_all(outgoing, "sp", split_axis=0, concat_axis=0, tiled=True)
    routed_rows, token_rows = (
        lax.all_gather(arrived, "tp", axis=0, tiled=True),
        lax.all_gather(normed, "tp", axis=0, tiled=True),
    )
    gate_part = jnp.einsum(
        "aecd,edf->aecf", routed_rows, w_exp_gate, preferred_element_type=jnp.float32
    )
    up_part = jnp.einsum(
        "aecd,edf->aecf", routed_rows, w_exp_up, preferred_element_type=jnp.float32
    )
    hidden = (jax.nn.silu(gate_part) * up_part).astype(jnp.bfloat16)
    expert_part = jnp.einsum(
        "aecf,efd->aecd", hidden, w_exp_down, preferred_element_type=jnp.float32
    )
    shared_gate = jnp.dot(token_rows, w_shared_gate, preferred_element_type=jnp.float32)
    shared_up = jnp.dot(token_rows, w_shared_up, preferred_element_type=jnp.float32)
    shared_hidden = (jax.nn.silu(shared_gate) * shared_up).astype(jnp.bfloat16)
    shared_part = jnp.dot(shared_hidden, w_shared_down, preferred_element_type=jnp.float32)
    expert_sum, shared_sum = (
        lax.psum_scatter(
            expert_part.astype(jnp.bfloat16), "tp", scatter_dimension=0, tiled=True
        ).astype(jnp.float32),
        lax.psum_scatter(
            shared_part.astype(jnp.bfloat16), "tp", scatter_dimension=0, tiled=True
        ).astype(jnp.float32),
    )
    returned = lax.all_to_all(
        expert_sum.astype(jnp.bfloat16), "sp", split_axis=0, concat_axis=0, tiled=True
    )
    returned = returned.reshape(experts * capacity, -1)
    picked = returned[slot_index].astype(jnp.float32).reshape(rows_local, top_k, -1)
    routed = jnp.sum(picked * route_weight[:, :, None], axis=1)
    shared_out = lax.optimization_barrier(shared_sum.astype(jnp.bfloat16))
    combined = routed + shared_out.astype(jnp.float32)
    return layer_norm(ALPHA * normed.astype(jnp.float32) + combined, norm_gain[1], norm_bias[1])


def solution(mesh):
    placed = (
        P(("sp", "tp"), None),
        P("sp", "tp"),
        P("sp", "tp"),
        P("sp", "tp"),
        P("tp"),
        P("tp", None),
        P(),
        P(),
        P(("sp", "tp"), None),
        P(("sp", "tp"), None),
        P("sp", None, "tp"),
        P("sp", None, "tp"),
        P("sp", "tp", None),
        P(None, "tp"),
        P(None, "tp"),
        P("tp", None),
    )
    return jax.shard_map(
        per_device, mesh=mesh, in_specs=placed, out_specs=P(("sp", "tp"), None), check_vma=False
    )
```

profile of v0, /device:TPU:1, one launch (start us, length us, event | category | flops | bytes accessed | tf_op | source)
XLA Modules:
  0.0 218.0 jit_solution(12864627702273954433)
XLA Ops:
  6.5 0.9 copy.41
  7.5 23.5 %all_gather.13 = bf16[1024,128]{0,1:T(8,128)(2,1)S(1)} all-gather(bf16[128,128]{0,1:T(8,128)(2,1)S(1)} %copy.41), channel_id=1, replica_groups=mesh['sp'=8,'tp'=4] {'sp'}, dimensions={0}, use_global_device_ids=true | all-gather | bytes 294912 | tf_op jit(solution)/shard_map/all_gather | solution.py:98
  31.0 25.1 %all_gather.14 = bf16[1024,128]{1,0:T(8,128)(2,1)S(1)} all-gather(bf16[128,128]{1,0:T(8,128)(2,1)} %param.22), channel_id=1, replica_groups=mesh['sp'=8,'tp'=4] {'sp'}, dimensions={0}, use_global_device_ids=true | all-gather | bytes 294912 | tf_op jit(solution)/shard_map/all_gather | solution.py:97
  56.1 0.9 copy.42
  57.0 0.1 copy.44
  57.2 3.2 %while.32 = (s32[]{:T(128)}, f32[1,2,128,8]{2,3,1,0:T(8,128)S(1)}, bf16[1024,1,128]{2,0,1:T(8,128)(2,1)S(1)}, bf16[128,1,2,128]{3,0,2,1:T(8,128)(2,1)S(1)}, f32[...) while((s32[]{:T(128)}, f32[1,2,128,8]{2,3,1,0:T(8,128)S(1)}, ...), condition=%wide.region_2.3_spmd.clone, body=%wide.region_0.2_spmd.clone.sunk | while | flops 35061380 | bytes 1394062 | solution.py:95
  57.2 0.1 broadcast_compare_fusion.5
  57.4 1.2 fusion.112
  58.6 0.1 dynamic_update_slice.12
  58.8 0.1 broadcast_compare_fusion.5
  59.0 1.2 fusion.112
  60.2 0.1 dynamic_update_slice.12
  60.4 9.9 %while.33 = (s32[]{:T(128)}, f32[128,1,2,128]{0,3,2,1:T(8,128)S(1)}, bf16[1024,1,128]{0,2,1:T(8,128)(2,1)S(1)}, bf16[1024,1,128]{2,0,1:T(8,128)(2,1)S(1)}, bf16[...) while((s32[]{:T(128)}, ...), condition=%wide.region_6.7_spmd.clone, body=%wide.region_4.6_spmd.clone.sunk | while | flops 88017024 | bytes 5658020 | solution.py:116
  60.4 0.2 broadcast_compare_fusion.6
  60.7 1.2 fusion.116
  61.9 2.4 %fusion.117 = f32[1,2,128,4,128]{2,3,4,1,0:T(4,128)S(1)} fusion(f32[1,2,128,4,128]{2,4,3,1,0:T(8,128)S(1)} %bitcast.200), kind=kOutput, calls=%fused_computation.36.clone.1 | output fusion | flops 16646144 | bytes 1048576 | tf_op jit(solution)/shard_map/while/body/eval_jaxpr/reduce_window_sum | solution.py:42
  64.3 0.8 fusion.118
  65.1 0.2 fusion.119
  65.4 0.2 broadcast_compare_fusion.6
  65.6 1.2 fusion.116
  66.8 2.4 %fusion.117 = f32[1,2,128,4,128]{2,3,4,1,0:T(4,128)S(1)} fusion(f32[1,2,128,4,128]{2,4,3,1,0:T(8,128)S(1)} %bitcast.200), kind=kOutput, calls=%fused_computation.36.clone.1 | output fusion | flops 16646144 | bytes 1048576 | tf_op jit(solution)/shard_map/while/body/eval_jaxpr/reduce_window_sum | solution.py:42
  69.2 0.8 fusion.118
  70.0 0.2 fusion.119
  70.3 2.4 %convolution_convert_fusion.2 = bf16[128,2048]{1,0:T(8,128)(2,1)} fusion(bf16[128,256]{0,1:T(8,128)(2,1)S(1)} %bitcast.205, bf16[256,2048]{1,0:T(8,128)(2,1)} %param.25), kind=kOutput, calls=%fused_computation.55 | convolution fusion | flops 134479872 | bytes 1638400 | tf_op jit(solution)/shard_map/dot_general | solution.py:120
  72.7 0.0 all-gather.2.cloned.1.call-start
  72.8 0.1 copy.46
  72.9 0.1 copy.45
  73.0 0.1 mul.157
  73.1 0.1 eq.15
  73.2 0.1 fusion.76
  73.3 0.1 reduce_window_sum.41
  73.4 0.2 select_reduce_fusion
  73.6 0.8 scatter_custom_fusion
  74.4 0.1 broadcast_in_dim.89
  74.6 29.5 %reduce-scatter.6.cloned.1.call-done = bf16[32,2048]{1,0:T(8,128)(2,1)} async-done(((bf16[128,2048]{1,0:T(8,128)(2,1)}), bf16[32,2048]{1,0:T(8,128)(2,1)}) %reduce-scatter.6.cloned.1.call-update) | async-done | bytes 131088 | tf_op jit(solution)/shard_map/reduce_scatter | solution.py:119
  104.0 1.1 fusion.68
  105.1 1.1 multiply_reduce_fusion.2
  106.2 1.0 add_convert_fusion.1
  107.2 0.8 gather_fusion
  108.1 0.1 gather.10
  108.2 0.1 select_bitcast_fusion
  108.3 18.7 %all_to_all.10 = bf16[8,1,12,2048]{3,2,1,0:T(8,128)(2,1)S(1)} all-to-all(bf16[8,1,12,2048]{3,2,1,0:T(8,128)(2,1)S(1)} %select_bitcast_fusion), channel_id=1, replica_groups=mesh['sp'=8,'tp'=4] {'sp'}, dimensions={0} | all-to-all | bytes 786432 | tf_op jit(solution)/shard_map/all_to_all | solution.py:142
  127.0 1.0 copy.48
  128.0 0.0 reduce-scatter.10.cloned.1.call-start
  128.0 19.3 %all-gather.2.cloned.1.call-done = bf16[32,1,12,2048]{3,0,2,1:T(8,128)(2,1)} async-done(((bf16[8,1,12,2048]{3,0,2,1:T(8,128)(2,1)}), bf16[32,1,12,2048]{3,0,2,1:T(8,128)(2,1)}) %all-gather.2.cloned.1.call-update) | async-done | bytes 1572880 | tf_op jit(solution)/shard_map/all_gather | solution.py:144
  147.4 2.4 %fusion.40 = f32[32,1,12,256]{3,0,2,1:T(8,128)S(1)} fusion(bf16[32,1,12,2048]{3,0,2,1:T(8,128)(2,1)} %all-gather.2.cloned.1.call-done, bf16[1,2048,256]{2,1,0:T(8,128)(2,1)} %param.30), kind=kOutput, calls=%fused_computation.60 | convolution fusion | flops 402653184 | bytes 3014656 | tf_op jit(solution)/shard_map/aecd,edf->aecf/dot_general | solution.py:147
  149.8 4.2 %fusion.85 = bf16[4,8,12,2048]{3,1,0,2:T(8,128)(2,1)} fusion(bf16[1,256,2048]{2,1,0:T(8,128)(2,1)S(1)} %copy-done, bf16[32,1,12,2048]{3,0,2,1:T(8,128)(2,1)S(1)} %copy-done.1, bf16[1,2048,256]{2,1,0:T(8,128)(2,1)} %param.31, f32[32,1,12,256]{3,0,2,1:T(8,128)S(1)} %fusion.40), kind=kOutput, calls=%fused_computation.117 | convolution fusion | flops 806682624 | bytes 5636096 | tf_op jit(solution)/shard_map/aecf,efd->aecd/dot_general | solution.py:154
  154.0 2.7 %copy.54 = bf16[4,8,12,2048]{3,1,2,0:T(8,128)(2,1)} copy(bf16[4,8,12,2048]{3,1,0,2:T(8,128)(2,1)} %fusion.85) | data formatting | bytes 3145728
  156.7 0.0 reduce-scatter.8.cloned.1.call-start
  156.8 7.4 %all_gather.16 = bf16[128,2048]{1,0:T(8,128)(2,1)S(1)} all-gather(bf16[32,2048]{1,0:T(8,128)(2,1)S(1)} %add_convert_fusion.1), channel_id=1, replica_groups=mesh['sp'=8,'tp'=4] {'tp'}, dimensions={0}, use_global_device_ids=true | all-gather | bytes 655360 | tf_op jit(solution)/shard_map/all_gather | solution.py:145
  164.2 1.6 fusion.92
  165.8 2.8 %convolution_convert_fusion.1 = bf16[128,2048]{1,0:T(8,128)(2,1)} fusion(bf16[256,2048]{1,0:T(8,128)(2,1)S(1)} %copy-done.4, bf16[128,2048]{1,0:T(8,128)(2,1)S(1)} %all_gather.16, bf16[2048,256]{1,0:T(8,128)(2,1)} %param.34, f32[128,256]{1,0:T(8,128)S(1)} %fusion.92), kind=kOutput, calls=%fused_computation.54 | convolution fusion | flops 268894208 | bytes 3276800 | tf_op jit(solution)/shard_map/dot_general | solution.py:160
  168.7 15.7 %reduce-scatter.10.cloned.1.call-done = bf16[8,24576]{1,0:T(8,128)(2,1)} async-done(((bf16[32,24576]{1,0:T(8,128)(2,1)}), bf16[8,24576]{1,0:T(8,128)(2,1)}) %reduce-scatter.10.cloned.1.call-update) | async-done | bytes 393232
  184.4 2.0 copy.49
  186.4 5.2 %all-to-all-start.1 = ((bf16[8,1,12,2048]{3,2,1,0:T(8,128)(2,1)}), bf16[8,1,12,2048]{3,2,1,0:T(8,128)(2,1)S(1)}, u32[]{:S(2)}, u32[]{:S(2)}) async-start(bf16[8,1,12,2048]{3,2,1,0:T(8,128)(2,1)} %copy.49), calls=%async_computation.2 | async-start | bytes 1048576 | tf_op jit(solution)/shard_map/all_to_all | solution.py:169
  191.6 0.1 copy.50
  191.7 16.7 %reduce-scatter.8.cloned.1.call-done = bf16[32,2048]{1,0:T(8,128)(2,1)} async-done(((bf16[128,2048]{1,0:T(8,128)(2,1)}), bf16[32,2048]{1,0:T(8,128)(2,1)}) %reduce-scatter.8.cloned.1.call-update) | async-done | bytes 131088 | tf_op jit(solution)/shard_map/reduce_scatter | solution.py:165
  208.4 0.1 reshape.324
  208.5 0.7 gather_fusion.1
  209.3 0.3 reshape.325
  209.6 0.7 multiply_reduce_fusion
  210.3 0.2 fusion.82
  210.5 0.2 multiply_reduce_fusion.1
  210.7 0.8 add_convert_fusion
  (58 shorter events, 0.5 us)
Async XLA Ops:
  6.5 143.2 %copy-start = (bf16[1,256,2048]{2,1,0:T(8,128)(2,1)S(1)}, bf16[1,256,2048]{2,1,0:T(8,128)(2,1)}, u32[]{:S(2)}) copy-start(bf16[1,256,2048]{2,1,0:T(8,128)(2,1)} %param.32) | copy-start | bytes 3145732
  6.5 97.5 %reduce-scatter.6.cloned.1.call-start = ((), (), s32[]{:S(2)}) async-start(), calls=%async_computation.5 | async-start | bytes 655360 | tf_op jit(solution)/shard_map/reduce_scatter | solution.py:119
  70.3 2.5 %copy-start.7 = (s32[32,2]{0,1:T(2,128)S(1)}, s32[32,2]{0,1:T(2,128)}, u32[]{:S(2)}) copy-start(s32[32,2]{0,1:T(2,128)} %param.28) | copy-start | bytes 772
  70.3 4.2 %copy-start.5 = (f32[2,2048]{1,0:T(2,128)S(1)}, f32[2,2048]{1,0:T(2,128)}, u32[]{:S(2)}) copy-start(f32[2,2048]{1,0:T(2,128)} %param.27) | copy-start | bytes 49156
  70.3 4.2 %copy-start.6 = (f32[2,2048]{1,0:T(2,128)S(1)}, f32[2,2048]{1,0:T(2,128)}, u32[]{:S(2)}) copy-start(f32[2,2048]{1,0:T(2,128)} %param.26) | copy-start | bytes 49156
  70.3 33.7 %copy-start.2 = (bf16[32,2048]{1,0:T(8,128)(2,1)S(1)}, bf16[32,2048]{1,0:T(8,128)(2,1)}, u32[]{:S(2)}) copy-start(bf16[32,2048]{1,0:T(8,128)(2,1)} %param.20) | copy-start | bytes 393220
  72.7 74.6 %all-gather.2.cloned.1.call-start = ((), (), s32[]{:S(2)}) async-start(), calls=%async_computation.6 | async-start | bytes 1966080 | tf_op jit(solution)/shard_map/all_gather | solution.py:144
  128.0 56.4 %reduce-scatter.10.cloned.1.call-start = ((), (), s32[]{:S(2)}) async-start(), calls=%async_computation.8 | async-start | bytes 1966080
  147.4 2.4 %copy-start.1 = (bf16[32,1,12,2048]{3,0,2,1:T(8,128)(2,1)S(1)}, bf16[32,1,12,2048]{3,0,2,1:T(8,128)(2,1)}, u32[]{:S(2)}) copy-start(bf16[32,1,12,2048]{3,0,2,1:T(8,128)(2,1)} %all-gather.2.cloned.1.call-done) | copy-start | bytes 4718596
  156.7 9.1 %copy-start.4 = (bf16[256,2048]{1,0:T(8,128)(2,1)S(1)}, bf16[256,2048]{1,0:T(8,128)(2,1)}, u32[]{:S(2)}) copy-start(bf16[256,2048]{1,0:T(8,128)(2,1)} %param.35) | copy-start | bytes 3145732
  156.7 51.7 %reduce-scatter.8.cloned.1.call-start = ((), (), s32[]{:S(2)}) async-start(), calls=%async_computation.7 | async-start | bytes 655360 | tf_op jit(solution)/shard_map/reduce_scatter | solution.py:165
  168.6 23.0 %copy-start.8 = (f32[32,2]{0,1:T(2,128)S(1)}, f32[32,2]{0,1:T(2,128)}, u32[]{:S(2)}) copy-start(f32[32,2]{0,1:T(2,128)} %param.29) | copy-start | bytes 772
  186.4 22.0 %all-to-all-start.1 = ((bf16[8,1,12,2048]{3,2,1,0:T(8,128)(2,1)}), bf16[8,1,12,2048]{3,2,1,0:T(8,128)(2,1)S(1)}, u32[]{:S(2)}, u32[]{:S(2)}) async-start(bf16[8,1,12,2048]{3,2,1,0:T(8,128)(2,1)} %copy.49), calls=%async_computation.2 | async-start | bytes 1048576 | tf_op jit(solution)/shard_map/all_to_all | solution.py:169
  208.5 1.8 copy-start.3
Sparse Core Ops, SparseCore 0:
  72.9 31.1 reduce-scatter.5
  128.1 19.2 all-gather.1
  156.8 27.5 reduce-scatter.9
  186.7 21.6 reduce-scatter.7
where the time goes:
time: 219 us; the launch traced here: 218 us
  waiting for transfers between devices  81.3 us (37%)
  blocking collectives  74.7 us (34%)
  matrix products  18.5 us (8%)
  between operations  13.4 us (6%)
  other arithmetic  12.7 us (6%)
  local copies, waits for them, and re-layouts  11.6 us (5%)
  starting transfers between devices  5.36 us (2%)
    reduce_scatter x1, waiting for transfers between devices, per_device(): lax.psum_scatter(jnp.dot(attended, w_out, preferred_element_type=jnp.floa...  29.5 us
    all_gather x1, blocking collectives, per_device(): lax.all_gather(key_rows, 'sp', axis=0, tiled=True).reshape(-1, kv_local, DH)  25.1 us
    all_gather x1, blocking collectives, per_device(): lax.all_gather(value_rows, 'sp', axis=0, tiled=True)  23.5 us
    all_gather x1, waiting for transfers between devices, per_device(): lax.all_gather(arrived, 'tp', axis=0, tiled=True)  19.3 us
    all_to_all x1, blocking collectives, per_device(): lax.all_to_all(outgoing, 'sp', split_axis=0, concat_axis=0, tiled=True)  18.7 us
    reduce_scatter x1, waiting for transfers between devices, per_device(): lax.psum_scatter(shared_part.astype(jnp.bfloat16), 'tp', scatter_dimensio...  16.7 us
    unnamed x5, waiting for transfers between devices  15.8 us
    all_gather x1, blocking collectives, per_device(): lax.all_gather(normed, 'tp', axis=0, tiled=True)  7.41 us
  transfers between devices with their start and end apart: 5, of which 4 were waited for; matrix products, arithmetic and copies ran while one was open for 4% of the time, Pallas kernels for 0%

commit v1 on v0

v1 whole, which is shorter than its diff:
```python
import functools

import jax
import jax.numpy as jnp
from jax import lax
from jax.experimental import pallas as pl
from jax.experimental.pallas import tpu as pltpu
from jax.sharding import PartitionSpec as P

DH = 128
ALPHA = 8.0**0.25
LN_EPS = 1e-05
BF = jnp.bfloat16
F32 = jnp.float32
MESH = pl.DeviceIdType.MESH


def dot(a, b):
    return jnp.dot(a, b, preferred_element_type=F32)


def silu_mul(g, u):
    return (g / (1.0 + jnp.exp(-g)) * u).astype(BF)


def layer_norm(x0, x1, gain, bias):
    width = x0.shape[1]
    total = 2 * width
    mean = (jnp.sum(x0, axis=1, keepdims=True) + jnp.sum(x1, axis=1, keepdims=True)) / total
    x0, x1 = x0 - mean, x1 - mean
    spread = (
        jnp.sum(x0 * x0, axis=1, keepdims=True) + jnp.sum(x1 * x1, axis=1, keepdims=True)
    ) / total
    inv = lax.rsqrt(spread + LN_EPS)
    n0 = (x0 * inv * gain[:, :width] + bias[:, :width]).astype(BF)
    n1 = (x1 * inv * gain[:, width:] + bias[:, width:]).astype(BF)
    return n0, n1


def kernel(
    cfg, res, q, k, v, off, wout, gain, bias, routing, rw, wg, wu, wd, sg, su, sd, out,
    wout_v, wg_v, wu_v, wd_v, sg_v, su_v, sd_v,
    kbuf, vbuf, acc, beyond, pj, r1, ys1, yr1, mixh, resall, rall, rwall,
    tok, outg, xb, yb, rb, ry, zb, ret, spart, rs, rsy, fin,
    wsem, ksend, krecv, vsend, vrecv, dsend, drecv, ysend, yrecv, asend, arecv,
    bsend, brecv, y3send, y3recv, zsend, zrecv, msend, mrecv,
):
    n, cap2, rows = cfg
    i, t = lax.axis_index("sp"), lax.axis_index("tp")
    c, y = lax.rem(t, 2), lax.div(t, 2)
    oc, oy = 1 - c, 1 - y
    mate, across = t + 1 - 2 * c, t + 2 - 4 * y
    shard = q.shape[0]
    half = out.shape[1] // 2
    pair = 2 * rows

    weights = [
        pltpu.make_async_copy(src, dst, wsem.at[a])
        for a, (src, dst) in enumerate(
            [(wout, wout_v), (sg, sg_v), (su, su_v), (sd, sd_v),
             (wg.at[0], wg_v), (wu.at[0], wu_v), (wd.at[0], wd_v)]
        )
    ]
    for cp in weights:
        cp.start()

    barrier = pltpu.get_barrier_semaphore()

    def hello(d, _):
        pl.semaphore_signal(
            barrier, inc=1, device_id={"sp": lax.rem(i + d, n), "tp": t}, device_id_type=MESH
        )
        return 0

    lax.fori_loop(1, n, hello, 0)
    for peer in (mate, across):
        pl.semaphore_signal(barrier, inc=1, device_id={"sp": i, "tp": peer}, device_id_type=MESH)
    pl.semaphore_wait(barrier, n + 1)

    def rcopy(src, dst, ssem, rsem, sp, tp):
        return pltpu.make_async_remote_copy(
            src_ref=src, dst_ref=dst, send_sem=ssem, recv_sem=rsem,
            device_id={"sp": sp, "tp": tp}, device_id_type=MESH,
        )

    def small(m, src, dst, peer):
        return rcopy(src, dst, msend.at[m], mrecv.at[m], i, peer)

    def kcopy(dest, slot):
        return rcopy(k, kbuf.at[slot], ksend.at[dest], krecv.at[slot], dest, t)

    def vcopy(dest, slot):
        return rcopy(v, vbuf.at[slot], vsend.at[dest], vrecv.at[slot], dest, t)

    def push(d, _):
        kcopy(i + d, i).start()
        vcopy(i + d, i).start()
        return 0

    lax.fori_loop(1, n - i, push, 0)
    m_res = small(0, res, resall.at[c], mate)
    m_rou = small(1, routing, rall.at[c], mate)
    m_rw = small(2, rw, rwall.at[c], mate)
    for cp in (m_res, m_rou, m_rw):
        cp.start()
    resall[c] = res[...]
    rall[c] = routing[...]
    rwall[c] = rw[...]

    heads = q.shape[1] // DH
    hq = heads * shard
    q2 = jnp.concatenate([q[:, h * DH:(h + 1) * DH] for h in range(heads)], axis=0)
    row = lax.broadcasted_iota(jnp.int32, (hq, shard), 0)
    col = lax.broadcasted_iota(jnp.int32, (hq, shard), 1)
    offs = jnp.full((hq, shard), off[0], F32)
    for h in range(1, heads):
        offs = jnp.where(row >= h * shard, off[h], offs)
    trow = lax.broadcasted_iota(jnp.int32, (shard, shard), 0)
    tcol = lax.broadcasted_iota(jnp.int32, (shard, shard), 1)
    later = jnp.where(trow > tcol, 1.0, 0.0).astype(BF)
    scale = DH**-0.5

    def stick(kb, vb, causal, prior):
        s = lax.dot_general(q2, kb, (((1,), (1,)), ((), ())), preferred_element_type=F32)
        s = s * scale + offs
        soft = jnp.maximum(s, 0.0) + jnp.log(1.0 + jnp.exp(-jnp.abs(s)))
        left = -soft if causal is None else jnp.where(causal, -soft, 0.0)
        hi = left.astype(BF)
        lo = (left - hi.astype(F32)).astype(BF)
        within = dot(hi, later) + dot(lo, later)
        w = jnp.exp(s - soft + within + prior)
        if causal is not None:
            w = jnp.where(causal, w, 0.0)
        total = jnp.sum(left, axis=1, keepdims=True)
        return dot(w.astype(BF), vb), total

    o, total = stick(k[...], v[...], col < lax.rem(row, shard), 0.0)
    acc[...] = o
    beyond[...] = jnp.broadcast_to(total, (hq, shard))

    def block(d, _):
        src = i - d
        kcopy(i, src).wait_recv()
        vcopy(i, src).wait_recv()
        o, total = stick(kbuf[src], vbuf[src], None, beyond[...])
        acc[...] += o
        beyond[...] += total
        return 0

    lax.fori_loop(1, i + 1, block, 0)
    att = jnp.concatenate(
        [acc[h * shard:(h + 1) * shard, :] for h in range(heads)], axis=1
    ).astype(BF)

    weights[0].wait()

    def project(h):
        columns = pl.ds(pl.multiple_of(h * half, half), half)
        pj[h] = dot(att, wout_v[:, columns]).astype(BF)

    project(oc)
    m_pj = small(3, pj.at[oc], r1, mate)
    m_pj.start()
    project(c)
    m_pj.wait_recv()
    mine_rows = pl.ds(pl.multiple_of(y * pair, pair), pair)
    other_rows = pl.ds(pl.multiple_of(oy * pair, pair), pair)
    ys1[...] = (pj[c, other_rows, :].astype(F32) + r1[other_rows, :].astype(F32)).astype(BF)
    m_y1 = small(4, ys1, yr1, across)
    m_y1.start()

    m_rou.wait_recv()
    m_rw.wait_recv()
    width = n * cap2
    rt = jnp.concatenate([rall[0], rall[1]], axis=0)
    rt0, rt1 = rt[:, 0:1], rt[:, 1:2]
    wt = jnp.concatenate([rwall[0], rwall[1]], axis=0)
    wcol = lax.broadcasted_iota(jnp.int32, (pair, width), 1)
    e_of = lax.div(wcol, cap2)
    r_of = wcol - e_of * cap2
    is0, is1 = rt0 == e_of, rt1 == e_of
    named = jnp.where(is0 | is1, 1.0, 0.0)
    before = jnp.where(
        lax.broadcasted_iota(jnp.int32, (pair, pair), 0)
        > lax.broadcasted_iota(jnp.int32, (pair, pair), 1), 1.0, 0.0
    ).astype(BF)
    rank = dot(before, named.astype(BF))
    place = jnp.where(rank == r_of.astype(F32), named, 0.0)
    back = place * jnp.where(is0, wt[:, 0:1], wt[:, 1:2])
    place_t = place.T.astype(BF)

    m_y1.wait_recv()
    mixh[c] = (
        pj[c, mine_rows, :].astype(F32) + r1[mine_rows, :].astype(F32) + yr1[...].astype(F32)
    )
    m_mix = small(5, mixh.at[c], mixh.at[c], mate)
    m_mix.start()
    m_res.wait_recv()
    small(5, mixh.at[oc], mixh.at[oc], mate).wait_recv()
    resid = jnp.concatenate([resall[0], resall[1]], axis=0)
    n0, n1 = layer_norm(
        ALPHA * resid[:, :half].astype(F32) + mixh[0],
        ALPHA * resid[:, half:].astype(F32) + mixh[1],
        gain[0:1, :], bias[0:1, :],
    )
    tok[y, 0] = n0
    tok[y, 1] = n1
    m_tok = small(6, tok.at[y, c], tok.at[y, c], across)
    m_tok.start()

    chosen = dot(place_t, tok[y, c])
    for e in range(n):
        outg[e] = chosen[e * cap2:(e + 1) * cap2, :].astype(BF)

    def dcopy(dest, slot):
        return rcopy(
            outg.at[dest], xb.at[c, y, slot], dsend.at[dest], drecv.at[slot], dest, t
        )

    def send_out(d, _):
        dcopy(lax.rem(i + d, n), i).start()
        return 0

    lax.fori_loop(1, n, send_out, 0)
    xb[c, y, i] = outg[i]

    def ycopy(slot, yy):
        ref = xb.at[c, yy, slot]
        return rcopy(ref, ref, ysend.at[slot], yrecv.at[slot], i, across)

    def acopy(slot, cc):
        ref = xb.at[cc, y, slot]
        return rcopy(ref, ref, asend.at[slot], arecv.at[slot], i, mate)

    def bcopy(slot, cc):
        ref = xb.at[cc, oy, slot]
        return rcopy(ref, ref, bsend.at[slot], brecv.at[slot], i, mate)

    def forward(slot):
        ycopy(slot, y).start()
        acopy(slot, c).start()

    forward(i)
    small(6, tok.at[oy, c], tok.at[oy, c], across).wait_recv()
    m_tok2 = small(7, tok.at[oy, c], tok.at[oy, c], mate)
    m_tok2.start()

    def relay(d, _):
        src = lax.rem(i + n - d, n)
        dcopy(i, src).wait_recv()
        forward(src)
        return 0

    lax.fori_loop(1, n, relay, 0)

    small(7, tok.at[oy, oc], tok.at[oy, oc], mate).wait_recv()
    for cp in weights[1:4]:
        cp.wait()
    t0 = jnp.concatenate([tok[0, 0], tok[1, 0]], axis=0)
    t1 = jnp.concatenate([tok[0, 1], tok[1, 1]], axis=0)
    gate = dot(t0, sg_v[:half, :]) + dot(t1, sg_v[half:, :])
    up = dot(t0, su_v[:half, :]) + dot(t1, su_v[half:, :])
    hid = silu_mul(gate, up)
    for h in range(2):
        spart[h] = dot(hid, sd_v[:, h * half:(h + 1) * half]).astype(BF)
    m_sp = small(8, spart.at[oc], rs, mate)
    m_sp.start()

    def relay2(d, _):
        src = lax.rem(i + n - d, n)
        ycopy(src, oy).wait_recv()
        bcopy(src, c).start()
        return 0

    lax.fori_loop(0, n, relay2, 0)
    m_sp.wait_recv()
    ys1s = (spart[c, other_rows, :].astype(F32) + rs[other_rows, :].astype(F32)).astype(BF)
    spart[c, other_rows, :] = ys1s
    m_sy = small(9, spart.at[c, other_rows, :], rsy, across)
    m_sy.start()

    def gathered(d, _):
        src = lax.rem(i + n - d, n)
        acopy(src, oc).wait_recv()
        bcopy(src, oc).wait_recv()
        return 0

    lax.fori_loop(0, n, gathered, 0)
    for cp in weights[4:]:
        cp.wait()
    count = 2 * n * cap2
    hidden = []
    for yy in range(2):
        x0 = xb[0, yy].astype(F32).reshape(n * cap2, half).astype(BF)
        x1 = xb[1, yy].astype(F32).reshape(n * cap2, half).astype(BF)
        gate = dot(x0, wg_v[:half, :]) + dot(x1, wg_v[half:, :])
        up = dot(x0, wu_v[:half, :]) + dot(x1, wu_v[half:, :])
        hidden.append(silu_mul(gate, up))
    hid = jnp.concatenate(hidden, axis=0)

    def down(h):
        columns = pl.ds(pl.multiple_of(h * half, half), half)
        part = dot(hid, wd_v[:, columns]).reshape(2, n, cap2, half)
        yb[h] = part.astype(BF)

    down(oc)
    m_yb0 = small(10, yb.at[oc, oy], rb.at[oy], mate)
    m_yb1 = small(11, yb.at[oc, y], rb.at[y], mate)
    m_yb0.start()
    m_yb1.start()
    down(c)

    def y3copy(slot):
        return rcopy(
            yb.at[c, oy, slot], ry.at[slot], y3send.at[slot], y3recv.at[slot], i, across
        )

    def zcopy(dest, slot):
        return rcopy(zb.at[dest], ret.at[slot], zsend.at[dest], zrecv.at[slot], dest, t)

    small(10, yb.at[oc, oy], rb.at[oy], mate).wait_recv()

    def fold(d, _):
        j = lax.rem(i + d, n)
        yb[c, oy, j] = (yb[c, oy, j].astype(F32) + rb[oy, j].astype(F32)).astype(BF)
        y3copy(j).start()
        return 0

    lax.fori_loop(1, n + 1, fold, 0)
    small(11, yb.at[oc, y], rb.at[y], mate).wait_recv()

    def fold2(d, _):
        j = lax.rem(i + d, n)
        y3copy(j).wait_recv()
        zb[j] = (
            yb[c, y, j].astype(F32) + rb[y, j].astype(F32) + ry[j].astype(F32)
        ).astype(BF)
        zcopy(j, i).start()
        return 0

    lax.fori_loop(1, n, fold2, 0)
    y3copy(i).wait_recv()
    ret[i] = (yb[c, y, i].astype(F32) + rb[y, i].astype(F32) + ry[i].astype(F32)).astype(BF)

    m_sy.wait_recv()
    shared = (
        spart[c, mine_rows, :].astype(F32) + rs[mine_rows, :].astype(F32) + rsy[...].astype(F32)
    ).astype(BF).astype(F32)
    b_hi = back.astype(BF)
    b_lo = (back - b_hi.astype(F32)).astype(BF)

    def returned(d, _):
        zcopy(i, lax.rem(i + n - d, n)).wait_recv()
        return 0

    lax.fori_loop(1, n, returned, 0)
    rows_back = ret[...].astype(F32).reshape(width, half).astype(BF)
    m_mix.wait_send()
    mixh[0] = shared + dot(b_hi, rows_back) + dot(b_lo, rows_back)
    own = pl.ds(pl.multiple_of(c * rows, rows), rows)
    theirs = pl.ds(pl.multiple_of(oc * rows, rows), rows)
    fin[2] = mixh[0, theirs, :]
    fin[c] = mixh[0, own, :]
    m_fin = small(12, fin.at[2], fin.at[c], mate)
    m_fin.start()
    small(12, fin.at[2], fin.at[oc], mate).wait_recv()
    n0, n1 = layer_norm(
        ALPHA * tok[y, 0, own, :].astype(F32) + fin[0],
        ALPHA * tok[y, 1, own, :].astype(F32) + fin[1],
        gain[1:2, :], bias[1:2, :],
    )
    out[:, :half] = n0
    out[:, half:] = n1

    def sent_kv(d, _):
        kcopy(i + d, i).wait_send()
        vcopy(i + d, i).wait_send()
        return 0

    lax.fori_loop(1, n - i, sent_kv, 0)

    def sent(d, _):
        j = lax.rem(i + d, n)
        dcopy(j, i).wait_send()
        zcopy(j, i).wait_send()
        return 0

    lax.fori_loop(1, n, sent, 0)

    def sent_all(j, _):
        ycopy(j, y).wait_send()
        acopy(j, c).wait_send()
        bcopy(j, c).wait_send()
        y3copy(j).wait_send()
        return 0

    lax.fori_loop(0, n, sent_all, 0)
    for cp in (m_res, m_rou, m_rw, m_pj, m_y1, m_tok, m_tok2, m_sp, m_sy, m_yb0, m_yb1, m_fin):
        cp.wait_send()


def per_device(
    residual, query_rows, key_rows, value_rows, head_offset, w_out, norm_gain, norm_bias,
    routing, route_weight, w_exp_gate, w_exp_up, w_exp_down, w_shared_gate, w_shared_up,
    w_shared_down,
):
    n = lax.axis_size("sp")
    rows, width = residual.shape
    shard = query_rows.shape[0]
    half = width // 2
    heads = query_rows.shape[1] // DH
    ff = w_exp_gate.shape[2]
    sff = w_shared_gate.shape[1]
    pair = 2 * rows
    experts = n * w_exp_gate.shape[0]
    assert w_exp_gate.shape[0] == 1 and key_rows.shape[1] == DH and lax.axis_size("tp") == 4
    cap = max(2, 3 * rows * routing.shape[1] // (2 * experts))
    cap2 = -(-2 * cap // 8) * 8
    vm = pl.BlockSpec(memory_space=pltpu.VMEM)
    anyw = pl.BlockSpec(memory_space=pl.ANY)
    smem = pl.BlockSpec(memory_space=pltpu.SMEM)
    dma = pltpu.SemaphoreType.DMA
    V = pltpu.VMEM
    scratch = [
        V(w_out.shape, BF), V(w_exp_gate.shape[1:], BF), V(w_exp_up.shape[1:], BF),
        V(w_exp_down.shape[1:], BF), V(w_shared_gate.shape, BF), V(w_shared_up.shape, BF),
        V(w_shared_down.shape, BF),
        V((n, shard, DH), BF), V((n, shard, DH), BF),
        V((heads * shard, DH), F32), V((heads * shard, shard), F32),
        V((2, shard, half), BF), V((shard, half), BF),
        V((pair, half), BF), V((pair, half), BF),
        V((2, pair, half), F32), V((2, rows, width), BF),
        V((2,) + routing.shape, jnp.int32), V((2,) + route_weight.shape, F32),
        V((2, 2, pair, half), BF),
        V((n, cap2, half), BF),
        V((2, 2, n, cap2, half), BF),
        V((2, 2, n, cap2, half), BF),
        V((2, n, cap2, half), BF),
        V((n, cap2, half), BF), V((n, cap2, half), BF), V((n, cap2, half), BF),
        V((2, shard, half), BF), V((shard, half), BF), V((pair, half), BF),
        V((3, rows, half), F32),
        dma((7,)),
    ] + [dma((n,))] * 16 + [dma((13,)), dma((13,))]
    return pl.pallas_call(
        functools.partial(kernel, (n, cap2, rows)),
        out_shape=jax.ShapeDtypeStruct(residual.shape, BF),
        in_specs=[vm, vm, vm, vm, smem, anyw, vm, vm, vm, vm] + [anyw] * 6,
        out_specs=vm,
        scratch_shapes=scratch,
        compiler_params=pltpu.CompilerParams(
            collective_id=0, has_side_effects=True, vmem_limit_bytes=56 * 1024 * 1024
        ),
    )(
        residual, query_rows, key_rows, value_rows, head_offset, w_out, norm_gain, norm_bias,
        routing, route_weight, w_exp_gate, w_exp_up, w_exp_down, w_shared_gate, w_shared_up,
        w_shared_down,
    )


def solution(mesh):
    placed = (
        P(("sp", "tp"), None),
        P("sp", "tp"),
        P("sp", "tp"),
        P("sp", "tp"),
        P("tp"),
        P("tp", None),
        P(),
        P(),
        P(("sp", "tp"), None),
        P(("sp", "tp"), None),
        P("sp", None, "tp"),
        P("sp", None, "tp"),
        P("sp", "tp", None),
        P(None, "tp"),
        P(None, "tp"),
        P("tp", None),
    )
    return jax.shard_map(
        per_device, mesh=mesh, in_specs=placed, out_specs=P(("sp", "tp"), None), check_vma=False
    )
```

time: 219 us -> 66.4 us (0.30)
  waiting for transfers between devices: 81.3 us -> 0 us
  blocking collectives: 74.7 us -> 0 us
  Pallas kernels: 0 us -> 62.6 us
  matrix products: 18.5 us -> 0 us
  between operations: 13.4 us -> 0.01 us
  other arithmetic: 12.7 us -> 0 us
  local copies, waits for them, and re-layouts: 11.6 us -> 3.63 us
  starting transfers between devices: 5.36 us -> 0 us
    pallas_call x0 -> x1, Pallas kernels: none -> 62.6 us  [per_device(): pl.pallas_call(functools.partial(kernel, (n, cap2, rows)), out_shape=jax....]
    all_gather x3 -> x0, blocking collectives: 56 us -> none  [the longest x1 25.1 us: per_device(): lax.all_gather(key_rows, 'sp', axis=0, tiled=True).reshape(-1, kv_local, DH)]
    reduce_scatter x2 -> x0, waiting for transfers between devices: 46.1 us -> none  [the longest x1 29.5 us: per_device(): lax.psum_scatter(jnp.dot(attended, w_out, preferred_element_type=jnp.floa...]
    all_gather x1 -> x0, waiting for transfers between devices: 19.3 us -> none  [per_device(): lax.all_gather(arrived, 'tp', axis=0, tiled=True)]
    all_to_all x1 -> x0, blocking collectives: 18.7 us -> none  [per_device(): lax.all_to_all(outgoing, 'sp', split_axis=0, concat_axis=0, tiled=True)]
    dot_general x11 -> x0, matrix products: 18.5 us -> none  [the longest x4 4.71 us: stick_terms(): jnp.einsum('tkgd,skd->kgts', queries, keys_block, preferred_element_type=...]
    unnamed x5 -> x0, waiting for transfers between devices: 15.8 us -> none
    all_to_all x1 -> x0, starting transfers between devices: 5.23 us -> none  [per_device(): lax.all_to_all(expert_sum.astype(jnp.bfloat16), 'sp', split_axis=0, conca...]
  transfers between devices with their start and end apart: 5 -> 0, of which waited for: 4 -> 0; matrix products, arithmetic and copies ran while one was open for 4% -> 0% of each run, Pallas kernels for 0% -> 0%
where the time goes in v1:
time: 66.4 us; the launch traced here: 66.2 us
  Pallas kernels  62.6 us (94%)
  local copies, waits for them, and re-layouts  3.63 us (5%)
    pallas_call x1, Pallas kernels, per_device(): pl.pallas_call(functools.partial(kernel, (n, cap2, rows)), out_shape=jax....  62.6 us
    unnamed x5, local copies, waits for them, and re-layouts  3.63 us

profile of v1, /device:TPU:1, one launch (start us, length us, event | category | flops | bytes accessed | tf_op | source)
XLA Modules:
  0.0 66.2 jit_solution(13555607332561405453)
XLA Ops:
  0.0 0.0 copy-start
  0.0 1.4 %copy.17.routing = s32[32,2]{1,0:T(8,128)} copy(s32[32,2]{0,1:T(2,128)} %param.24) | data formatting | bytes 512 | tf_op args[8]
  1.4 0.0 copy-done
  1.4 0.7 %copy.18.rw = f32[32,2]{1,0:T(8,128)} copy(f32[32,2]{0,1:T(2,128)S(1)} %copy-done) | data formatting | bytes 512 | tf_op args[9]
  2.1 62.6 %shard_map.154 = bf16[32,2048]{1,0:T(8,128)(2,1)} custom-call(bf16[32,2048]{1,0:T(8,128)(2,1)} %res.1, bf16[128,256]{1,0:T(8,128)(2,1)} %q.1, bf16[128,128]{1,0:T(8,128)(2,1)} %k.1, bf16[128,128]{1,0:T(8,128)(2,1)} %v.1, f32[2]{0:T(128)} %off.1, bf16[256,2048]{1,0:T(8,128)(2,1)} %wout.1, f32[2,2048]{1,0:T(2,128)} %gain.1, f32[2,2048]{1,0:T(2,128)} %bias.1, ...), custom_call_target="tpu_custom_call" | custom-call | tf_op jit(solution)/shard_map/pallas_call | solution.py:444
  64.6 1.6 %copy.20 = bf16[32,2048]{1,0:T(8,128)(2,1)} copy(bf16[32,2048]{1,0:T(8,128)(2,1)} %shard_map.154) | data formatting | bytes 262144
Async XLA Ops:
  0.0 1.4 %copy-start = (f32[32,2]{0,1:T(2,128)S(1)}, f32[32,2]{0,1:T(2,128)}, u32[]{:S(2)}) copy-start(f32[32,2]{0,1:T(2,128)} %param.25) | copy-start | bytes 772

commit v2 on v1

--- a/solution.py
+++ b/solution.py
@@ -43,9 +43,9 @@
     kbuf, vbuf, acc, beyond, pj, r1, ys1, yr1, mixh, resall, rall, rwall,
     tok, outg, xb, yb, rb, ry, zb, ret, spart, rs, rsy, fin,
     wsem, ksend, krecv, vsend, vrecv, dsend, drecv, ysend, yrecv, asend, arecv,
-    bsend, brecv, y3send, y3recv, zsend, zrecv, msend, mrecv,
+    bsend, brecv, y3send, y3recv, zsend, zrecv, msend, mrecv, fksend, fvsend,
 ):
-    n, cap2, rows = cfg
+    n, cap2, rows, span = cfg
     i, t = lax.axis_index("sp"), lax.axis_index("tp")
     c, y = lax.rem(t, 2), lax.div(t, 2)
     oc, oy = 1 - c, 1 - y
@@ -75,7 +75,6 @@
     lax.fori_loop(1, n, hello, 0)
     for peer in (mate, across):
         pl.semaphore_signal(barrier, inc=1, device_id={"sp": i, "tp": peer}, device_id_type=MESH)
-    pl.semaphore_wait(barrier, n + 1)
 
     def rcopy(src, dst, ssem, rsem, sp, tp):
         return pltpu.make_async_remote_copy(
@@ -92,17 +91,34 @@
     def vcopy(dest, slot):
         return rcopy(v, vbuf.at[slot], vsend.at[dest], vrecv.at[slot], dest, t)
 
-    def push(d, _):
+    layer, lane = lax.div(i, span), lax.rem(i, span)
+
+    def forward_kv(slot, peer):
+        dest = layer * span + peer
+        kc = rcopy(kbuf.at[slot], kbuf.at[slot],
+                   fksend.at[slot, peer], krecv.at[slot], dest, t)
+        vc = rcopy(vbuf.at[slot], vbuf.at[slot],
+                   fvsend.at[slot, peer], vrecv.at[slot], dest, t)
+        return kc, vc
+
+    def push_lane(d, _):
         kcopy(i + d, i).start()
         vcopy(i + d, i).start()
         return 0
 
-    lax.fori_loop(1, n - i, push, 0)
+    def push_layer(d, _):
+        dest = (n // span - d) * span + lane
+        kcopy(dest, i).start()
+        vcopy(dest, i).start()
+        return 0
+
+    def push_all():
+        lax.fori_loop(1, span - lane, push_lane, 0)
+        lax.fori_loop(1, n // span - layer, push_layer, 0)
+
     m_res = small(0, res, resall.at[c], mate)
     m_rou = small(1, routing, rall.at[c], mate)
     m_rw = small(2, rw, rwall.at[c], mate)
-    for cp in (m_res, m_rou, m_rw):
-        cp.start()
     resall[c] = res[...]
     rall[c] = routing[...]
     rwall[c] = rw[...]
@@ -138,16 +154,53 @@
     acc[...] = o
     beyond[...] = jnp.broadcast_to(total, (hq, shard))
 
-    def block(d, _):
-        src = i - d
-        kcopy(i, src).wait_recv()
-        vcopy(i, src).wait_recv()
+    pl.semaphore_wait(barrier, n + 1)
+    push_all()
+    for cp in (m_res, m_rou, m_rw):
+        cp.start()
+
+    def block(src):
         o, total = stick(kbuf[src], vbuf[src], None, beyond[...])
         acc[...] += o
         beyond[...] += total
-        return 0
-
-    lax.fori_loop(1, i + 1, block, 0)
+
+    def arrive(src):
+        kcopy(i, src).wait_recv()
+        vcopy(i, src).wait_recv()
+
+    def own_layer(d, _):
+        arrive(i - d)
+        block(i - d)
+        return 0
+
+    lax.fori_loop(1, lane + 1, own_layer, 0)
+
+    def earlier_layer(d, _):
+        first = (layer - d) * span
+        direct = first + lane
+        arrive(direct)
+
+        def hand_on(p, _):
+            for cp in forward_kv(direct, lax.rem(lane + p, span)):
+                cp.start()
+            return 0
+
+        lax.fori_loop(1, span, hand_on, 0)
+
+        def one(p, _):
+            src = first + span - 1 - p
+
+            @pl.when(src != direct)
+            def _():
+                arrive(src)
+
+            block(src)
+            return 0
+
+        lax.fori_loop(0, span, one, 0)
+        return 0
+
+    lax.fori_loop(1, layer + 1, earlier_layer, 0)
     att = jnp.concatenate(
         [acc[h * shard:(h + 1) * shard, :] for h in range(heads)], axis=1
     ).astype(BF)
@@ -172,22 +225,21 @@
     m_rou.wait_recv()
     m_rw.wait_recv()
     width = n * cap2
-    rt = jnp.concatenate([rall[0], rall[1]], axis=0)
-    rt0, rt1 = rt[:, 0:1], rt[:, 1:2]
-    wt = jnp.concatenate([rwall[0], rwall[1]], axis=0)
-    wcol = lax.broadcasted_iota(jnp.int32, (pair, width), 1)
-    e_of = lax.div(wcol, cap2)
-    r_of = wcol - e_of * cap2
-    is0, is1 = rt0 == e_of, rt1 == e_of
+    rt = jnp.concatenate([rall[0], rall[1]], axis=1)
+    wt = jnp.concatenate([rwall[0], rwall[1]], axis=1)
+    wrow = lax.broadcasted_iota(jnp.int32, (width, pair), 0)
+    e_of = lax.div(wrow, cap2)
+    r_of = wrow - e_of * cap2
+    is0, is1 = rt[0:1, :] == e_of, rt[1:2, :] == e_of
     named = jnp.where(is0 | is1, 1.0, 0.0)
     before = jnp.where(
         lax.broadcasted_iota(jnp.int32, (pair, pair), 0)
-        > lax.broadcasted_iota(jnp.int32, (pair, pair), 1), 1.0, 0.0
+        < lax.broadcasted_iota(jnp.int32, (pair, pair), 1), 1.0, 0.0
     ).astype(BF)
-    rank = dot(before, named.astype(BF))
+    rank = dot(named.astype(BF), before)
     place = jnp.where(rank == r_of.astype(F32), named, 0.0)
-    back = place * jnp.where(is0, wt[:, 0:1], wt[:, 1:2])
-    place_t = place.T.astype(BF)
+    back = (place * jnp.where(is0, wt[0:1, :], wt[1:2, :])).T
+    place_t = place.astype(BF)
 
     m_y1.wait_recv()
     mixh[c] = (
@@ -251,7 +303,8 @@
         forward(src)
         return 0
 
-    lax.fori_loop(1, n, relay, 0)
+    early = n // 2
+    lax.fori_loop(1, early, relay, 0)
 
     small(7, tok.at[oy, oc], tok.at[oy, oc], mate).wait_recv()
     for cp in weights[1:4]:
@@ -265,6 +318,7 @@
         spart[h] = dot(hid, sd_v[:, h * half:(h + 1) * half]).astype(BF)
     m_sp = small(8, spart.at[oc], rs, mate)
     m_sp.start()
+    lax.fori_loop(early, n, relay, 0)
 
     def relay2(d, _):
         src = lax.rem(i + n - d, n)
@@ -272,43 +326,50 @@
         bcopy(src, c).start()
         return 0
 
-    lax.fori_loop(0, n, relay2, 0)
-    m_sp.wait_recv()
-    ys1s = (spart[c, other_rows, :].astype(F32) + rs[other_rows, :].astype(F32)).astype(BF)
-    spart[c, other_rows, :] = ys1s
-    m_sy = small(9, spart.at[c, other_rows, :], rsy, across)
-    m_sy.start()
-
-    def gathered(d, _):
-        src = lax.rem(i + n - d, n)
-        acopy(src, oc).wait_recv()
-        bcopy(src, oc).wait_recv()
-        return 0
-
-    lax.fori_loop(0, n, gathered, 0)
+    lax.fori_loop(0, early, relay2, 0)
+
+    def gathered_own(d, _):
+        acopy(lax.rem(i + n - d, n), oc).wait_recv()
+        return 0
+
+    lax.fori_loop(0, n, gathered_own, 0)
     for cp in weights[4:]:
         cp.wait()
-    count = 2 * n * cap2
-    hidden = []
-    for yy in range(2):
+
+    def expert(yy):
         x0 = xb[0, yy].astype(F32).reshape(n * cap2, half).astype(BF)
         x1 = xb[1, yy].astype(F32).reshape(n * cap2, half).astype(BF)
         gate = dot(x0, wg_v[:half, :]) + dot(x1, wg_v[half:, :])
         up = dot(x0, wu_v[:half, :]) + dot(x1, wu_v[half:, :])
-        hidden.append(silu_mul(gate, up))
-    hid = jnp.concatenate(hidden, axis=0)
-
-    def down(h):
+        return silu_mul(gate, up)
+
+    def down(hid, yy, h):
         columns = pl.ds(pl.multiple_of(h * half, half), half)
-        part = dot(hid, wd_v[:, columns]).reshape(2, n, cap2, half)
-        yb[h] = part.astype(BF)
-
-    down(oc)
+        yb[h, yy] = dot(hid, wd_v[:, columns]).reshape(n, cap2, half).astype(BF)
+
+    hid = expert(y)
+    down(hid, y, oc)
+    m_yb1 = small(11, yb.at[oc, y], rb.at[y], mate)
+    m_yb1.start()
+    down(hid, y, c)
+    lax.fori_loop(early, n, relay2, 0)
+    m_sp.wait_recv()
+    spart[c, other_rows, :] = (
+        spart[c, other_rows, :].astype(F32) + rs[other_rows, :].astype(F32)
+    ).astype(BF)
+    m_sy = small(9, spart.at[c, other_rows, :], rsy, across)
+    m_sy.start()
+
+    def gathered(d, _):
+        bcopy(lax.rem(i + n - d, n), oc).wait_recv()
+        return 0
+
+    lax.fori_loop(0, n, gathered, 0)
+    hid = expert(oy)
+    down(hid, oy, oc)
     m_yb0 = small(10, yb.at[oc, oy], rb.at[oy], mate)
-    m_yb1 = small(11, yb.at[oc, y], rb.at[y], mate)
     m_yb0.start()
-    m_yb1.start()
-    down(c)
+    down(hid, oy, c)
 
     def y3copy(slot):
         return rcopy(
@@ -372,12 +433,29 @@
     out[:, :half] = n0
     out[:, half:] = n1
 
-    def sent_kv(d, _):
+    def sent_lane(d, _):
         kcopy(i + d, i).wait_send()
         vcopy(i + d, i).wait_send()
         return 0
 
-    lax.fori_loop(1, n - i, sent_kv, 0)
+    def sent_layer(d, _):
+        dest = (n // span - d) * span + lane
+        kcopy(dest, i).wait_send()
+        vcopy(dest, i).wait_send()
+        return 0
+
+    def sent_on(d, _):
+        def to_peer(p, _):
+            for cp in forward_kv((layer - d) * span + lane, lax.rem(lane + p, span)):
+                cp.wait_send()
+            return 0
+
+        lax.fori_loop(1, span, to_peer, 0)
+        return 0
+
+    lax.fori_loop(1, span - lane, sent_lane, 0)
+    lax.fori_loop(1, n // span - layer, sent_layer, 0)
+    lax.fori_loop(1, layer + 1, sent_on, 0)
 
     def sent(d, _):
         j = lax.rem(i + d, n)
@@ -416,6 +494,7 @@
     assert w_exp_gate.shape[0] == 1 and key_rows.shape[1] == DH and lax.axis_size("tp") == 4
     cap = max(2, 3 * rows * routing.shape[1] // (2 * experts))
     cap2 = -(-2 * cap // 8) * 8
+    span = max(s for s in range(1, n + 1) if n % s == 0 and s * s <= n)
     vm = pl.BlockSpec(memory_space=pltpu.VMEM)
     anyw = pl.BlockSpec(memory_space=pl.ANY)
     smem = pl.BlockSpec(memory_space=pltpu.SMEM)
@@ -430,7 +509,7 @@
         V((2, shard, half), BF), V((shard, half), BF),
         V((pair, half), BF), V((pair, half), BF),
         V((2, pair, half), F32), V((2, rows, width), BF),
-        V((2,) + routing.shape, jnp.int32), V((2,) + route_weight.shape, F32),
+        V((2,) + routing.shape[::-1], jnp.int32), V((2,) + route_weight.shape[::-1], F32),
         V((2, 2, pair, half), BF),
         V((n, cap2, half), BF),
         V((2, 2, n, cap2, half), BF),
@@ -440,9 +519,9 @@
         V((2, shard, half), BF), V((shard, half), BF), V((pair, half), BF),
         V((3, rows, half), F32),
         dma((7,)),
-    ] + [dma((n,))] * 16 + [dma((13,)), dma((13,))]
+    ] + [dma((n,))] * 16 + [dma((13,)), dma((13,)), dma((n, span)), dma((n, span))]
     return pl.pallas_call(
-        functools.partial(kernel, (n, cap2, rows)),
+        functools.partial(kernel, (n, cap2, rows, span)),
         out_shape=jax.ShapeDtypeStruct(residual.shape, BF),
         in_specs=[vm, vm, vm, vm, smem, anyw, vm, vm, vm, vm] + [anyw] * 6,
         out_specs=vm,
@@ -452,8 +531,8 @@
         ),
     )(
         residual, query_rows, key_rows, value_rows, head_offset, w_out, norm_gain, norm_bias,
-        routing, route_weight, w_exp_gate, w_exp_up, w_exp_down, w_shared_gate, w_shared_up,
-        w_shared_down,
+        routing.T, route_weight.T, w_exp_gate, w_exp_up, w_exp_down, w_shared_gate,
+        w_shared_up, w_shared_down,
     )
 
 

time: 66.4 us -> 65.8 us (level)
  local copies, waits for them, and re-layouts: 3.63 us -> 1.57 us
  Pallas kernels: 62.6 us -> 64 us
    unnamed x5 -> x1, local copies, waits for them, and re-layouts: 3.63 us -> 1.57 us
    pallas_call x1, Pallas kernels: 62.6 us -> 64 us  [per_device(): pl.pallas_call(functools.partial(kernel, (n, cap2, rows, span)), out_shap...]
where the time goes in v2:
time: 65.8 us; the launch traced here: 65.6 us
  Pallas kernels  64 us (97%)
  local copies, waits for them, and re-layouts  1.57 us (2%)
    pallas_call x1, Pallas kernels, per_device(): pl.pallas_call(functools.partial(kernel, (n, cap2, rows, span)), out_shap...  64 us
    unnamed x1, local copies, waits for them, and re-layouts  1.57 us

profile of v2, /device:TPU:1, one launch (start us, length us, event | category | flops | bytes accessed | tf_op | source)
XLA Modules:
  0.0 65.6 jit_solution(9935108424904923452)
XLA Ops:
  0.0 64.0 %shard_map.154 = bf16[32,2048]{1,0:T(8,128)(2,1)} custom-call(bf16[32,2048]{1,0:T(8,128)(2,1)} %res.1, bf16[128,256]{1,0:T(8,128)(2,1)} %q.1, bf16[128,128]{1,0:T(8,128)(2,1)} %k.1, bf16[128,128]{1,0:T(8,128)(2,1)} %v.1, f32[2]{0:T(128)} %off.1, bf16[256,2048]{1,0:T(8,128)(2,1)} %wout.1, f32[2,2048]{1,0:T(2,128)} %gain.1, f32[2,2048]{1,0:T(2,128)} %bias.1, ...), custom_call_target="tpu_custom_call" | custom-call | tf_op jit(solution)/shard_map/pallas_call | solution.py:523
  64.1 1.6 %copy.18 = bf16[32,2048]{1,0:T(8,128)(2,1)} copy(bf16[32,2048]{1,0:T(8,128)(2,1)} %shard_map.154) | data formatting | bytes 262144

commit v3 on v2

--- a/solution.py
+++ b/solution.py
@@ -44,6 +44,7 @@
     tok, outg, xb, yb, rb, ry, zb, ret, spart, rs, rsy, fin,
     wsem, ksend, krecv, vsend, vrecv, dsend, drecv, ysend, yrecv, asend, arecv,
     bsend, brecv, y3send, y3recv, zsend, zrecv, msend, mrecv, fksend, fvsend,
+    y0send, y0recv, comb,
 ):
     n, cap2, rows, span = cfg
     i, t = lax.axis_index("sp"), lax.axis_index("tp")
@@ -211,13 +212,15 @@
         columns = pl.ds(pl.multiple_of(h * half, half), half)
         pj[h] = dot(att, wout_v[:, columns]).astype(BF)
 
+    mine_rows = pl.ds(pl.multiple_of(y * pair, pair), pair)
+    other_rows = pl.ds(pl.multiple_of(oy * pair, pair), pair)
     project(oc)
-    m_pj = small(3, pj.at[oc], r1, mate)
+    m_pj = small(3, pj.at[oc, other_rows, :], r1.at[other_rows, :], mate)
+    m_pj2 = small(13, pj.at[oc, mine_rows, :], r1.at[mine_rows, :], mate)
     m_pj.start()
+    m_pj2.start()
     project(c)
     m_pj.wait_recv()
-    mine_rows = pl.ds(pl.multiple_of(y * pair, pair), pair)
-    other_rows = pl.ds(pl.multiple_of(oy * pair, pair), pair)
     ys1[...] = (pj[c, other_rows, :].astype(F32) + r1[other_rows, :].astype(F32)).astype(BF)
     m_y1 = small(4, ys1, yr1, across)
     m_y1.start()
@@ -241,18 +244,19 @@
     back = (place * jnp.where(is0, wt[0:1, :], wt[1:2, :])).T
     place_t = place.astype(BF)
 
+    m_pj2.wait_recv()
     m_y1.wait_recv()
     mixh[c] = (
         pj[c, mine_rows, :].astype(F32) + r1[mine_rows, :].astype(F32) + yr1[...].astype(F32)
-    )
+    ).astype(BF)
     m_mix = small(5, mixh.at[c], mixh.at[c], mate)
     m_mix.start()
     m_res.wait_recv()
     small(5, mixh.at[oc], mixh.at[oc], mate).wait_recv()
     resid = jnp.concatenate([resall[0], resall[1]], axis=0)
     n0, n1 = layer_norm(
-        ALPHA * resid[:, :half].astype(F32) + mixh[0],
-        ALPHA * resid[:, half:].astype(F32) + mixh[1],
+        ALPHA * resid[:, :half].astype(F32) + mixh[0].astype(F32),
+        ALPHA * resid[:, half:].astype(F32) + mixh[1].astype(F32),
         gain[0:1, :], bias[0:1, :],
     )
     tok[y, 0] = n0
@@ -367,8 +371,17 @@
     lax.fori_loop(0, n, gathered, 0)
     hid = expert(oy)
     down(hid, oy, oc)
-    m_yb0 = small(10, yb.at[oc, oy], rb.at[oy], mate)
-    m_yb0.start()
+
+    def y0copy(slot):
+        return rcopy(
+            yb.at[oc, oy, slot], rb.at[oy, slot], y0send.at[slot], y0recv.at[slot], i, mate
+        )
+
+    def swap_out(d, _):
+        y0copy(lax.rem(i + d, n)).start()
+        return 0
+
+    lax.fori_loop(1, n + 1, swap_out, 0)
     down(hid, oy, c)
 
     def y3copy(slot):
@@ -379,10 +392,10 @@
     def zcopy(dest, slot):
         return rcopy(zb.at[dest], ret.at[slot], zsend.at[dest], zrecv.at[slot], dest, t)
 
-    small(10, yb.at[oc, oy], rb.at[oy], mate).wait_recv()
 
     def fold(d, _):
         j = lax.rem(i + d, n)
+        y0copy(j).wait_recv()
         yb[c, oy, j] = (yb[c, oy, j].astype(F32) + rb[oy, j].astype(F32)).astype(BF)
         y3copy(j).start()
         return 0
@@ -416,12 +429,11 @@
 
     lax.fori_loop(1, n, returned, 0)
     rows_back = ret[...].astype(F32).reshape(width, half).astype(BF)
-    m_mix.wait_send()
-    mixh[0] = shared + dot(b_hi, rows_back) + dot(b_lo, rows_back)
+    comb[...] = shared + dot(b_hi, rows_back) + dot(b_lo, rows_back)
     own = pl.ds(pl.multiple_of(c * rows, rows), rows)
     theirs = pl.ds(pl.multiple_of(oc * rows, rows), rows)
-    fin[2] = mixh[0, theirs, :]
-    fin[c] = mixh[0, own, :]
+    fin[2] = comb[theirs, :]
+    fin[c] = comb[own, :]
     m_fin = small(12, fin.at[2], fin.at[c], mate)
     m_fin.start()
     small(12, fin.at[2], fin.at[oc], mate).wait_recv()
@@ -470,10 +482,13 @@
         acopy(j, c).wait_send()
         bcopy(j, c).wait_send()
         y3copy(j).wait_send()
+        y0copy(j).wait_send()
         return 0
 
     lax.fori_loop(0, n, sent_all, 0)
-    for cp in (m_res, m_rou, m_rw, m_pj, m_y1, m_tok, m_tok2, m_sp, m_sy, m_yb0, m_yb1, m_fin):
+    for cp in (
+        m_res, m_rou, m_rw, m_pj, m_pj2, m_y1, m_mix, m_tok, m_tok2, m_sp, m_sy, m_yb1, m_fin
+    ):
         cp.wait_send()
 
 
@@ -508,7 +523,7 @@
         V((heads * shard, DH), F32), V((heads * shard, shard), F32),
         V((2, shard, half), BF), V((shard, half), BF),
         V((pair, half), BF), V((pair, half), BF),
-        V((2, pair, half), F32), V((2, rows, width), BF),
+        V((2, pair, half), BF), V((2, rows, width), BF),
         V((2,) + routing.shape[::-1], jnp.int32), V((2,) + route_weight.shape[::-1], F32),
         V((2, 2, pair, half), BF),
         V((n, cap2, half), BF),
@@ -519,7 +534,9 @@
         V((2, shard, half), BF), V((shard, half), BF), V((pair, half), BF),
         V((3, rows, half), F32),
         dma((7,)),
-    ] + [dma((n,))] * 16 + [dma((13,)), dma((13,)), dma((n, span)), dma((n, span))]
+    ] + [dma((n,))] * 16 + [dma((14,)), dma((14,)), dma((n, span)), dma((n, span))] + [
+        dma((n,)), dma((n,)), V((pair, half), F32)
+    ]
     return pl.pallas_call(
         functools.partial(kernel, (n, cap2, rows, span)),
         out_shape=jax.ShapeDtypeStruct(residual.shape, BF),

time: 65.8 us -> 66 us (level)
  no operation moved by 1% of the time
where the time goes in v3:
time: 66 us; the launch traced here: 65.9 us
  Pallas kernels  64.3 us (97%)
  local copies, waits for them, and re-layouts  1.57 us (2%)
    pallas_call x1, Pallas kernels, per_device(): pl.pallas_call(functools.partial(kernel, (n, cap2, rows, span)), out_shap...  64.3 us
    unnamed x1, local copies, waits for them, and re-layouts  1.57 us

profile of v3, /device:TPU:1, one launch (start us, length us, event | category | flops | bytes accessed | tf_op | source)
XLA Modules:
  0.0 65.9 jit_solution(3098672724085368020)
XLA Ops:
  0.0 64.3 %shard_map.154 = bf16[32,2048]{1,0:T(8,128)(2,1)} custom-call(bf16[32,2048]{1,0:T(8,128)(2,1)} %res.1, bf16[128,256]{1,0:T(8,128)(2,1)} %q.1, bf16[128,128]{1,0:T(8,128)(2,1)} %k.1, bf16[128,128]{1,0:T(8,128)(2,1)} %v.1, f32[2]{0:T(128)} %off.1, bf16[256,2048]{1,0:T(8,128)(2,1)} %wout.1, f32[2,2048]{1,0:T(2,128)} %gain.1, f32[2,2048]{1,0:T(2,128)} %bias.1, ...), custom_call_target="tpu_custom_call" | custom-call | tf_op jit(solution)/shard_map/pallas_call | solution.py:540
  64.3 1.6 %copy.18 = bf16[32,2048]{1,0:T(8,128)(2,1)} copy(bf16[32,2048]{1,0:T(8,128)(2,1)} %shard_map.154) | data formatting | bytes 262144
